TPU v7x, 32 devices: a whole 2x2x4 slice. The times are simulated.
32 devices in a mesh: grp: 2 (over y), sp: 4 (over z), tp: 4 (over x, core).
Axes of the slice: x: 2, y: 2, z: 4, core: 2. Of those that a mesh axis runs over, the one named last changes fastest.
Arguments:
- target: bfloat16 [1024, 2048], P(('grp', 'sp', 'tp')), parts along dimension 0, may hold values from -5 to 5
- source: bfloat16 [8192, 2048], P(('grp', 'sp', 'tp')), parts along dimension 0, may hold values from -5 to 5
- source_gain: float32 [2048], replicated, may hold values from 0.1 to 1.9
- pre_first: float32 [2048], replicated, may hold values from 0.1 to 1.9
- query_first: bfloat16 [2048, 2048], P(None, 'tp')
- keyval_first: bfloat16 [2048, 1024], P(None, 'tp')
- out_first: bfloat16 [2048, 2048], P('tp'), may hold values from -0.125 to 0.125
- post_first: float32 [2048], replicated, may hold values from 0.1 to 1.9
- ffn_pre: float32 [2048], replicated, may hold values from 0.1 to 1.9
- w_gate: bfloat16 [2048, 2816], P(None, 'tp'), may hold values from -0.125 to 0.125
- w_value: bfloat16 [2048, 2816], P(None, 'tp'), may hold values from -0.125 to 0.125
- conv_gate: float32 [3, 2816], P(None, 'tp'), may hold values from -3.5 to 3.5
- conv_value: float32 [3, 2816], P(None, 'tp'), may hold values from -3.5 to 3.5
- w_down: bfloat16 [2816, 2048], P('tp'), may hold values from -0.109375 to 0.109375
- ffn_post: float32 [2048], replicated, may hold values from 0.1 to 1.9
- pre_second: float32 [2048], replicated, may hold values from 0.1 to 1.9
- query_second: bfloat16 [2048, 2048], P(None, 'tp')
- keyval_second: bfloat16 [2048, 1024], P(None, 'tp')
- out_second: bfloat16 [2048, 2048], P('tp'), may hold values from -0.125 to 0.125
- post_second: float32 [2048], replicated, may hold values from 0.1 to 1.9
Outputs:
- decoded: float32 [1024, 2048], P(('grp', 'sp', 'tp')), parts along dimension 0
There are 2 independent parts, one for each index of `grp`. A program takes and returns all parts, laid end to end along the dimension named above; an argument that names none is the same for every part. Nothing has to cross between parts.
All inputs are finite; a program needn't handle non-finite values.
Results may differ from a plain program's by a relative error of at most 0.04.
Values may be sent and summed in bfloat16 or wider, within the bound.
A program may use at most 128 MiB of HBM per device.

v0:
```python
import math

import jax
import jax.numpy as jnp
from jax import lax
from jax.experimental import pallas as pl
from jax.experimental.pallas import tpu as pltpu
from jax.sharding import PartitionSpec as P

HEAD = 128
CHUNKS = 4
PIECES = 2
EXP_SCALE = HEAD ** (-0.5) * math.log2(math.e)
F32, BF16 = jnp.float32, jnp.bfloat16
MESH = pl.DeviceIdType.MESH


def normed(values, gain):
    widened = values.astype(F32)
    return widened * lax.rsqrt(jnp.mean(widened * widened, axis=-1, keepdims=True) + 1e-06) * gain


def times(start, stop, body):
    if stop - start <= 4:
        for index in range(start, stop):
            body(index)
    else:

        @pl.loop(start, stop)
        def _(index):
            body(index)


def dot(left, right):
    return jnp.dot(left, right, preferred_element_type=F32)


def decoder_kernel(
    n_tp,
    n_sp,
    target_h,
    source_h,
    source_gain,
    pre_first,
    query_first_h,
    keyval_first_h,
    out_first_h,
    post_first,
    ffn_pre,
    gate_h,
    value_h,
    conv_gate,
    conv_value,
    down_h,
    ffn_post,
    pre_second,
    query_second_h,
    keyval_second_h,
    out_second_h,
    post_second,
    decoded,
    target_v,
    source_v,
    query_first,
    keyval_first,
    out_first,
    w_gate,
    w_value,
    w_down,
    query_second,
    keyval_second,
    out_second,
    local_sem,
    hidden,
    hidden_send,
    hidden_recv,
    src,
    src_send,
    src_recv,
    q_slots,
    q_sem,
    k_first,
    v_first,
    k_second,
    v_second,
    kv_send,
    kv_recv,
    run_max,
    run_sum,
    run_out,
    mix_send,
    mix_recv,
    stat_send,
    stat_recv,
    mix_sem,
    part,
    pair_recv,
    pair_sum,
    part_recv,
    part_send,
    pair_sem,
    part_sem,
    halo_send,
    halo_recv,
    halo_sem,
    stream,
):
    me = lax.axis_index("tp")
    z = lax.axis_index("sp")
    sib = me + 1 - 2 * lax.rem(me, 2)
    core, chip = lax.rem(me, 2), me // 2
    n_chip = n_tp // 2
    rows = target_v.shape[0]
    width = target_v.shape[1]
    span = width // PIECES
    chunk = src.shape[2]
    block_rows = rows * n_tp

    def tp_at(distance):
        return lax.rem(me + distance, n_tp)

    def sp_at(distance):
        return lax.rem(z + distance, n_sp)

    def to_tp(source, dest, send, recv, device):
        return pltpu.make_async_remote_copy(
            src_ref=source, dst_ref=dest, send_sem=send, recv_sem=recv,
            device_id={"tp": device}, device_id_type=MESH,
        )

    def to_sp(source, dest, send, recv, device):
        return pltpu.make_async_remote_copy(
            src_ref=source, dst_ref=dest, send_sem=send, recv_sem=recv,
            device_id={"sp": device}, device_id_type=MESH,
        )

    pairs = [
        (target_h, target_v),
        (source_h, source_v),
        (query_first_h, query_first),
        (keyval_first_h, keyval_first),
        (keyval_second_h, keyval_second),
        (out_first_h, out_first),
        (gate_h, w_gate),
        (value_h, w_value),
        (down_h, w_down),
        (query_second_h, query_second),
        (out_second_h, out_second),
    ]
    loads = [
        pltpu.make_async_copy(a, b, local_sem.at[i]) for i, (a, b) in enumerate(pairs)
    ]
    for load in loads:
        load.start()

    barrier = pltpu.get_barrier_semaphore()
    for distance in range(1, n_tp):
        pl.semaphore_signal(barrier, inc=1, device_id={"tp": tp_at(distance)}, device_id_type=MESH)
    for distance in range(1, n_sp):
        pl.semaphore_signal(barrier, inc=1, device_id={"sp": sp_at(distance)}, device_id_type=MESH)
    pl.semaphore_wait(barrier, n_tp - 1 + n_sp - 1)

    def hidden_copy(phase, piece, slot, device):
        return to_tp(
            hidden.at[phase, piece, slot], hidden.at[phase, piece, slot],
            hidden_send.at[phase], hidden_recv.at[phase, piece, slot], device,
        )

    def gather_start(phase, value):
        for piece in range(PIECES):
            hidden[phase, piece, me] = value[:, piece * span : (piece + 1) * span].astype(BF16)
            for d in range(1, n_chip):
                hidden_copy(phase, piece, me, tp_at(2 * d)).start()
            hidden_copy(phase, piece, me, sib).start()

    def gather_times(phase, weights):
        totals = [None] * len(weights)
        for piece in range(PIECES + 1):
            if piece < PIECES:
                for d in range(1, n_chip):
                    slot = tp_at(2 * d)
                    hidden_copy(phase, piece, slot, sib).wait_recv()
                    hidden_copy(phase, piece, slot, sib).start()
            if piece == 0:
                continue
            ready = piece - 1
            for d in range(n_chip):
                slot = lax.rem(sib + 2 * d, n_tp)
                hidden_copy(phase, ready, slot, sib).wait_recv()
            whole = hidden[phase, ready]
            if rows % 16:
                whole = whole.astype(F32).reshape(block_rows, span).astype(BF16)
            else:
                whole = whole.reshape(block_rows, span)
            for index, weight in enumerate(weights):
                product = dot(whole, weight[ready * span : (ready + 1) * span, :])
                totals[index] = product if ready == 0 else totals[index] + product
        return totals

    def gather_drain(phase):
        for piece in range(PIECES):
            for _ in range(2 * n_chip - 1):
                hidden_copy(phase, piece, me, sib).wait_send()

    def pair_copy(phase, piece):
        return to_tp(
            part.at[phase, piece, 1 - core], pair_recv.at[phase, piece],
            part_send.at[phase, 0], pair_sem.at[phase, piece], sib,
        )

    def chip_copy(phase, piece, distance, slot):
        other = lax.rem(chip + distance, n_chip)
        return to_tp(
            pair_sum.at[phase, piece, other], part_recv.at[phase, piece, slot],
            part_send.at[phase, 1], part_sem.at[phase, piece, slot], 2 * other + core,
        )

    def scatter_sum(phase, left, weight):
        for piece in range(PIECES):
            product = dot(left, weight[:, piece * span : (piece + 1) * span])
            product = product.reshape(n_chip, 2, rows, span)
            for parity in range(2):
                part[phase, piece, parity] = product[:, parity].astype(BF16)
            pair_copy(phase, piece).start()
        for piece in range(PIECES):
            pair_copy(phase, piece).wait_recv()
            mine = part[phase, piece, core].astype(F32)
            pair_sum[phase, piece] = (mine + pair_recv[phase, piece].astype(F32)).astype(BF16)
            for d in range(1, n_chip):
                chip_copy(phase, piece, d, chip).start()
        sums = []
        for piece in range(PIECES):
            total = pair_sum[phase, piece, chip].astype(F32)
            for d in range(1, n_chip):
                slot = lax.rem(chip + d, n_chip)
                chip_copy(phase, piece, d, slot).wait_recv()
                total = total + part_recv[phase, piece, slot].astype(F32)
            sums.append(total)
        return jnp.concatenate(sums, axis=1)

    def sum_drain(phase):
        for piece in range(PIECES):
            pair_copy(phase, piece).wait_send()
            for d in range(1, n_chip):
                chip_copy(phase, piece, d, chip).wait_send()

    def head_columns(queries):
        blocks = [
            queries[:, h : h + HEAD].T for h in range(0, queries.shape[1], HEAD)
        ]
        return jnp.concatenate(blocks, axis=1).astype(BF16)

    def head_rows(columns):
        blocks = [
            columns[:, c : c + block_rows].T for c in range(0, columns.shape[1], block_rows)
        ]
        return jnp.concatenate(blocks, axis=1).astype(BF16)

    loads[0].wait()
    gather_start(0, normed(target_v[...], pre_first[...]))

    def src_copy(slot, c, device, kind):
        return to_tp(
            src.at[slot, c], src.at[slot, c], src_send.at[kind], src_recv.at[slot, c], device
        )

    loads[1].wait()
    for c in range(CHUNKS):
        src[me, c] = normed(source_v[pl.ds(c * chunk, chunk)], source_gain[...]).astype(BF16)
        for d in range(1, n_chip):
            src_copy(me, c, tp_at(2 * d), 0).start()
        src_copy(me, c, sib, 0).start()

    loads[2].wait()
    q_slots[z] = head_columns(gather_times(0, [query_first])[0])

    def q_copy(distance, slot):
        return to_sp(
            q_slots.at[z], q_slots.at[z] if slot is None else q_slots.at[slot],
            q_sem.at[0, 0], q_sem.at[1, z if slot is None else slot], sp_at(distance),
        )

    for d in range(1, n_sp):
        q_copy(d, None).start()

    loads[3].wait()
    loads[4].wait()

    def project(lines, block, offset):
        first = dot(lines, keyval_first[...])
        second = dot(lines, keyval_second[...])
        place = pl.ds(offset, lines.shape[0])
        k_first[block, place] = first[:, :HEAD].astype(BF16)
        v_first[block, place] = first[:, HEAD:].astype(BF16)
        k_second[z, block, place] = second[:, :HEAD].astype(BF16)
        v_second[z, block, place] = second[:, HEAD:].astype(BF16)

    def project_pair(block, c, mine, other):
        lines = jnp.concatenate([src[mine, c], src[other, c]], axis=0)
        project(lines, block, c * 2 * chunk)

    def absorb(keys, values, queries, slot, fresh):
        scores = dot(keys, queries)
        newest = jnp.max(scores, axis=0, keepdims=True)
        if not fresh:
            newest = jnp.maximum(newest, run_max[slot])
        weights = jnp.exp2((scores - newest) * EXP_SCALE)
        added = jnp.sum(weights, axis=0, keepdims=True)
        gathered = lax.dot_general(
            values, weights.astype(BF16), (((0,), (0,)), ((), ())), preferred_element_type=F32
        )
        if not fresh:
            rescale = jnp.exp2((run_max[slot] - newest) * EXP_SCALE)
            added = added + run_sum[slot] * rescale
            gathered = gathered + run_out[slot] * rescale
        run_max[slot] = newest
        run_sum[slot] = added
        run_out[slot] = gathered

    def absorb_block(block, fresh):
        @pl.loop(0, n_sp)
        def _(slot):
            absorb(k_first[block], v_first[block], q_slots[slot], slot, fresh)

    def kv_copies(block, slot, peer):
        return [
            to_sp(
                store.at[slot, block], store.at[slot, block],
                kv_send.at[index], kv_recv.at[index, slot, block], peer,
            )
            for index, store in enumerate((k_second, v_second))
        ]

    def kv_hop(block, hop, arrive=True, leave=True):
        for step in (1, -1):
            slot = z - step * (hop - 1)
            peer = z + step

            @pl.when(jnp.logical_and(slot >= 0, slot < n_sp))
            def _():
                if arrive:
                    for copy in kv_copies(block, slot, sp_at(1)):
                        copy.wait_recv()
                if leave:

                    @pl.when(jnp.logical_and(hop < n_sp, jnp.logical_and(peer >= 0, peer < n_sp)))
                    def _():
                        for copy in kv_copies(block, slot, peer):
                            copy.start()

    def kv_drain(block, hop):
        for step in (1, -1):
            slot = z - step * (hop - 1)
            peer = z + step
            inside = jnp.logical_and(slot >= 0, slot < n_sp)

            @pl.when(jnp.logical_and(inside, jnp.logical_and(peer >= 0, peer < n_sp)))
            def _():
                for copy in kv_copies(block, slot, peer):
                    copy.wait_send()

    for c in range(CHUNKS):
        src_copy(sib, c, sib, 0).wait_recv()
        project_pair(0, c, me, sib)
    for d in range(1, n_sp):
        q_copy(d, sp_at(d)).wait_recv()
    kv_hop(0, 1, arrive=False)
    absorb_block(0, True)

    def far_chip(d):
        near = tp_at(2 * d)
        far = lax.rem(sib + 2 * d, n_tp)
        for c in range(CHUNKS):
            src_copy(near, c, sib, 1).wait_recv()
            src_copy(near, c, sib, 1).start()
            src_copy(far, c, sib, 1).wait_recv()
            project_pair(d, c, near, far)

    def far_absorb(d):
        far_chip(d)
        absorb_block(d, False)

    times(1, n_chip - 1, far_absorb)
    last = n_chip - 1
    far_chip(last)

    def mix_copies(distance, slot):
        peer = sp_at(distance)
        return [
            to_sp(sent.at[peer], got.at[slot], mix_sem.at[index, 0, 0], mix_sem.at[index, 1, slot], peer)
            for index, (sent, got) in enumerate(((mix_send, mix_recv), (stat_send, stat_recv)))
        ]

    def finish_slot(slot, mixes, stats):
        absorb(k_first[last], v_first[last], q_slots[slot], slot, False)
        total = run_sum[slot]
        mixes[slot] = (run_out[slot] / total).astype(BF16)
        stats[slot] = jnp.concatenate([run_max[slot], total], axis=0)

    @pl.loop(1, n_sp)
    def _(d):
        finish_slot(sp_at(d), mix_send, stat_send)
        for copy in mix_copies(d, z):
            copy.start()

    finish_slot(z, mix_recv, stat_recv)
    for d in range(1, n_sp):
        for copy in mix_copies(d, sp_at(d)):
            copy.wait_recv()
    kv_hop(0, 2)
    for block in range(1, n_chip):
        kv_hop(block, 1, arrive=False)
    top = stat_recv[0, 0:1]
    for slot in range(1, n_sp):
        top = jnp.maximum(top, stat_recv[slot, 0:1])
    weight_sum = jnp.zeros_like(top)
    weighted = jnp.zeros(run_out.shape[1:], F32)
    for slot in range(n_sp):
        share = jnp.exp2((stat_recv[slot, 0:1] - top) * EXP_SCALE) * stat_recv[slot, 1:2]
        weight_sum = weight_sum + share
        weighted = weighted + mix_recv[slot].astype(F32) * share
    loads[5].wait()
    mixed = scatter_sum(0, head_rows(weighted / weight_sum), out_first)
    after_first = target_v[...].astype(F32) + normed(mixed, post_first[...])
    stream[...] = after_first

    gather_start(1, normed(after_first, ffn_pre[...]))
    kv_hop(0, 3)
    for block in range(1, n_chip):
        kv_hop(block, 2)
    loads[6].wait()
    loads[7].wait()
    up_gate, up_value = (up.astype(BF16) for up in gather_times(1, [w_gate, w_value]))
    halo_send[0] = up_gate[block_rows - 16 :]
    halo_send[1] = up_value[block_rows - 16 :]
    halo = to_sp(halo_send, halo_recv, halo_sem.at[0], halo_sem.at[1], sp_at(1))

    @pl.when(z < n_sp - 1)
    def _():
        halo.start()

    @pl.when(z > 0)
    def _():
        halo.wait_recv()

    def causal_mix(up_rows, rim, taps):
        here = up_rows.astype(F32)
        rim = jnp.where(z > 0, rim.astype(F32), 0.0)
        row = lax.broadcasted_iota(jnp.int32, here.shape, 0)
        before = jnp.where(row == 0, rim[15:16], pltpu.roll(here, 1, 0))
        earlier = jnp.where(
            row == 0, rim[14:15], jnp.where(row == 1, rim[15:16], pltpu.roll(here, 2, 0))
        )
        return taps[0:1] * earlier + taps[1:2] * before + taps[2:3] * here

    gated = (
        jax.nn.gelu(causal_mix(up_gate, halo_recv[0], conv_gate[...]), approximate=True)
        * causal_mix(up_value, halo_recv[1], conv_value[...])
    ).astype(BF16)
    loads[8].wait()
    ffn_sum = scatter_sum(1, gated, w_down)
    after_ffn = stream[...] + normed(ffn_sum, ffn_post[...])
    stream[...] = after_ffn

    gather_start(2, normed(after_ffn, pre_second[...]))
    for block in range(1, n_chip):
        kv_hop(block, 3)
    loads[9].wait()
    queries = head_columns(gather_times(2, [query_second])[0])
    for d in range(1, n_sp):
        q_copy(d, None).wait_send()
    q_slots[z] = queries

    for block in range(n_chip):
        absorb(k_second[z, block], v_second[z, block], q_slots[z], 0, block == 0)

    @pl.loop(4, max(n_sp, 4) + 1)
    def _(hop):
        for block in range(n_chip):
            kv_hop(block, hop)

    @pl.loop(1, n_sp)
    def _(d):
        slot = sp_at(d)
        for block in range(n_chip):
            absorb(k_second[slot, block], v_second[slot, block], q_slots[z], 0, False)

    loads[10].wait()
    mixed = scatter_sum(2, head_rows(run_out[0] / run_sum[0]), out_second)
    decoded[...] = stream[...] + normed(mixed, post_second[...])

    for phase in range(3):
        gather_drain(phase)
        sum_drain(phase)
    for c in range(CHUNKS):
        for _ in range(n_chip):
            src_copy(me, c, sib, 0).wait_send()
        for d in range(1, n_chip):
            src_copy(me, c, sib, 1).wait_send()

    def drain(d):
        for block in range(n_chip):
            kv_drain(block, d)
        for copy in mix_copies(d, z):
            copy.wait_send()

    times(1, n_sp, drain)

    @pl.when(z < n_sp - 1)
    def _():
        halo.wait_send()


def per_device(*arrays):
    (target, source, source_gain, pre_first, query_first, keyval_first, out_first, post_first,
     ffn_pre, w_gate, w_value, conv_gate, conv_value, w_down, ffn_post, pre_second,
     query_second, keyval_second, out_second, post_second) = arrays
    n_tp, n_sp = lax.axis_size("tp"), lax.axis_size("sp")
    sharers = 2 * HEAD // keyval_first.shape[1]
    if sharers > 1:
        groups = [list(range(low, low + sharers)) for low in range(0, n_tp, sharers)]
        keyval_first, keyval_second = (
            lax.all_gather(w, "tp", axis=1, tiled=True, axis_index_groups=groups)
            for w in (keyval_first, keyval_second)
        )
    rows, width = target.shape
    lines = source.shape[0]
    block_rows = rows * n_tp
    columns = query_first.shape[1] // HEAD * block_rows
    hidden_units = w_gate.shape[1]
    n_chip = n_tp // 2
    span = width // PIECES
    dma = pltpu.SemaphoreType.DMA
    any_spec = pl.BlockSpec(memory_space=pl.ANY)
    vmem = pl.BlockSpec(memory_space=pltpu.VMEM)

    def row(gain):
        return gain.reshape(1, width)

    scratch = [
        pltpu.VMEM(target.shape, BF16),
        pltpu.VMEM(source.shape, BF16),
        *(pltpu.VMEM(w.shape, BF16) for w in (
            query_first, keyval_first, out_first, w_gate, w_value, w_down,
            query_second, keyval_second, out_second)),
        dma((11,)),
        pltpu.VMEM((3, PIECES, n_tp, rows, span), BF16),
        dma((3,)),
        dma((3, PIECES, n_tp)),
        pltpu.VMEM((n_tp, CHUNKS, lines // CHUNKS, width), BF16),
        dma((2,)),
        dma((n_tp, CHUNKS)),
        pltpu.VMEM((n_sp, HEAD, columns), BF16),
        dma((2, n_sp)),
        pltpu.VMEM((n_chip, 2 * lines, HEAD), BF16),
        pltpu.VMEM((n_chip, 2 * lines, HEAD), BF16),
        pltpu.VMEM((n_sp, n_chip, 2 * lines, HEAD), BF16),
        pltpu.VMEM((n_sp, n_chip, 2 * lines, HEAD), BF16),
        dma((2,)),
        dma((2, n_sp, n_chip)),
        pltpu.VMEM((n_sp, 1, columns), F32),
        pltpu.VMEM((n_sp, 1, columns), F32),
        pltpu.VMEM((n_sp, HEAD, columns), F32),
        pltpu.VMEM((n_sp, HEAD, columns), BF16),
        pltpu.VMEM((n_sp, HEAD, columns), BF16),
        pltpu.VMEM((n_sp, 2, columns), F32),
        pltpu.VMEM((n_sp, 2, columns), F32),
        dma((2, 2, n_sp)),
        pltpu.VMEM((3, PIECES, 2, n_chip, rows, span), BF16),
        pltpu.VMEM((3, PIECES, n_chip, rows, span), BF16),
        pltpu.VMEM((3, PIECES, n_chip, rows, span), BF16),
        pltpu.VMEM((3, PIECES, n_chip, rows, span), BF16),
        dma((3, 2)),
        dma((3, PIECES)),
        dma((3, PIECES, n_chip)),
        pltpu.VMEM((2, 16, hidden_units), BF16),
        pltpu.VMEM((2, 16, hidden_units), BF16),
        dma((2,)),
        pltpu.VMEM((rows, width), F32),
    ]

    def kernel(*refs):
        decoder_kernel(n_tp, n_sp, *refs)

    return pl.pallas_call(
        kernel,
        out_shape=jax.ShapeDtypeStruct((rows, width), F32),
        in_specs=[any_spec, any_spec, vmem, vmem, any_spec, any_spec, any_spec, vmem, vmem,
                  any_spec, any_spec, vmem, vmem, any_spec, vmem, vmem, any_spec, any_spec,
                  any_spec, vmem],
        out_specs=vmem,
        scratch_shapes=scratch,
        compiler_params=pltpu.CompilerParams(
            collective_id=0, has_side_effects=True, vmem_limit_bytes=67_000_000
        ),
        name="decoder",
    )(
        target, source, row(source_gain), row(pre_first), query_first, keyval_first, out_first,
        row(post_first), row(ffn_pre), w_gate, w_value, conv_gate, conv_value, w_down,
        row(ffn_post), row(pre_second), query_second, keyval_second, out_second, row(post_second),
    )


def solution(mesh):
    rows = P(("grp", "sp", "tp"), None)
    by_column, by_row = P(None, "tp"), P("tp", None)
    placed = (
        rows, rows, P(), P(), by_column, by_column, by_row, P(), P(), by_column, by_column,
        by_column, by_column, by_row, P(), P(), by_column, by_column, by_row, P(),
    )
    return jax.shard_map(
        per_device, mesh=mesh, in_specs=placed, out_specs=rows, check_vma=False
    )
```

profile of v0, /device:TPU:30, one launch (start us, length us, event | category | flops | bytes accessed | tf_op | source)
XLA Modules:
  0.0 105.2 jit_solution(3147025750366289075)
XLA Ops:
  0.0 0.0 copy-start
  0.0 4.7 %copy.21.refs_9_ = bf16[2048,704]{1,0:T(8,128)(2,1)} copy(bf16[2048,704]{0,1:T(8,128)(2,1)} %param.29) | data formatting | bytes 5767168 | tf_op args[9]
  4.8 0.0 copy-done
  4.8 2.8 %copy.22.refs_10_ = bf16[2048,704]{1,0:T(8,128)(2,1)} copy(bf16[2048,704]{0,1:T(8,128)(2,1)S(1)} %copy-done) | data formatting | bytes 5767168 | tf_op args[10]
  7.6 96.0 %decoder.1 = f32[32,2048]{1,0:T(8,128)} custom-call(bf16[32,2048]{1,0:T(8,128)(2,1)} %refs_0_.1, bf16[256,2048]{1,0:T(8,128)(2,1)} %refs_1_.1, f32[1,2048]{1,0:T(1,128)} %bitcast.7, f32[1,2048]{1,0:T(1,128)} %bitcast.8, bf16[2048,512]{1,0:T(8,128)(2,1)} %refs_4_.1, bf16[2048,256]{1,0:T(8,128)(2,1)} %refs_5_.1, bf16[512,2048]{1,0:T(8,128)(2,1)} %refs_6_.1, ...), custom_call_target="tpu_custom_call" | custom-call | tf_op jit(solution)/shard_map/decoder/pallas_call | solution.py:585
  103.6 1.7 %copy.24 = f32[32,2048]{1,0:T(8,128)} copy(f32[32,2048]{1,0:T(8,128)} %decoder.1) | data formatting | bytes 524288
Async XLA Ops:
  0.0 4.8 %copy-start = (bf16[2048,704]{0,1:T(8,128)(2,1)S(1)}, bf16[2048,704]{0,1:T(8,128)(2,1)}, u32[]{:S(2)}) copy-start(bf16[2048,704]{0,1:T(8,128)(2,1)} %param.30) | copy-start | bytes 8650756
where the time goes:
time: 105 us
  Pallas kernels  96 us (91%)
  local copies, waits for them, and re-layouts  9.25 us (9%)
    pallas_call x1, Pallas kernels, per_device(): pl.pallas_call(kernel, out_shape=jax.ShapeDtypeStruct((rows, width), F32)...  96 us
    unnamed x5, local copies, waits for them, and re-layouts  9.25 us

commit v1 on v0

--- a/solution.py
+++ b/solution.py
@@ -18,6 +18,9 @@
 def normed(values, gain):
     widened = values.astype(F32)
     return widened * lax.rsqrt(jnp.mean(widened * widened, axis=-1, keepdims=True) + 1e-06) * gain
+
+
+SC = jax.named_scope
 
 
 def times(start, stop, body):
@@ -64,6 +67,8 @@
     query_first,
     keyval_first,
     out_first,
+    gate_t,
+    value_t,
     w_gate,
     w_value,
     w_down,
@@ -141,8 +146,8 @@
         (keyval_first_h, keyval_first),
         (keyval_second_h, keyval_second),
         (out_first_h, out_first),
-        (gate_h, w_gate),
-        (value_h, w_value),
+        (gate_h, gate_t),
+        (value_h, value_t),
         (down_h, w_down),
         (query_second_h, query_second),
         (out_second_h, out_second),
@@ -158,7 +163,17 @@
         pl.semaphore_signal(barrier, inc=1, device_id={"tp": tp_at(distance)}, device_id_type=MESH)
     for distance in range(1, n_sp):
         pl.semaphore_signal(barrier, inc=1, device_id={"sp": sp_at(distance)}, device_id_type=MESH)
-    pl.semaphore_wait(barrier, n_tp - 1 + n_sp - 1)
+    last_tp = n_tp - 1
+
+    @pl.when(jnp.logical_and(z > 0, me < last_tp))
+    def _():
+        pl.semaphore_signal(
+            barrier, inc=1, device_id={"sp": z - 1, "tp": last_tp}, device_id_type=MESH
+        )
+
+    gives_halo = jnp.logical_and(me == last_tp, z < n_sp - 1)
+    with SC("barrier"):
+        pl.semaphore_wait(barrier, n_tp - 1 + n_sp - 1 + jnp.where(gives_halo, n_tp - 1, 0))
 
     def hidden_copy(phase, piece, slot, device):
         return to_tp(
@@ -173,7 +188,7 @@
                 hidden_copy(phase, piece, me, tp_at(2 * d)).start()
             hidden_copy(phase, piece, me, sib).start()
 
-    def gather_times(phase, weights):
+    def gather_times(phase, weights, extra=None):
         totals = [None] * len(weights)
         for piece in range(PIECES + 1):
             if piece < PIECES:
@@ -192,6 +207,10 @@
                 whole = whole.astype(F32).reshape(block_rows, span).astype(BF16)
             else:
                 whole = whole.reshape(block_rows, span)
+            if extra is not None:
+                if ready == 0:
+                    rim = extra()
+                whole = jnp.concatenate([whole, rim[:, ready * span : (ready + 1) * span]], axis=0)
             for index, weight in enumerate(weights):
                 product = dot(whole, weight[ready * span : (ready + 1) * span, :])
                 totals[index] = product if ready == 0 else totals[index] + product
@@ -257,7 +276,8 @@
         return jnp.concatenate(blocks, axis=1).astype(BF16)
 
     loads[0].wait()
-    gather_start(0, normed(target_v[...], pre_first[...]))
+    with SC("norm0"):
+        gather_start(0, normed(target_v[...], pre_first[...]))
 
     def src_copy(slot, c, device, kind):
         return to_tp(
@@ -272,7 +292,8 @@
         src_copy(me, c, sib, 0).start()
 
     loads[2].wait()
-    q_slots[z] = head_columns(gather_times(0, [query_first])[0])
+    with SC("qproj"):
+        q_slots[z] = head_columns(gather_times(0, [query_first])[0])
 
     def q_copy(distance, slot):
         return to_sp(
@@ -286,18 +307,17 @@
     loads[3].wait()
     loads[4].wait()
 
-    def project(lines, block, offset):
-        first = dot(lines, keyval_first[...])
-        second = dot(lines, keyval_second[...])
-        place = pl.ds(offset, lines.shape[0])
-        k_first[block, place] = first[:, :HEAD].astype(BF16)
-        v_first[block, place] = first[:, HEAD:].astype(BF16)
-        k_second[z, block, place] = second[:, :HEAD].astype(BF16)
-        v_second[z, block, place] = second[:, HEAD:].astype(BF16)
-
-    def project_pair(block, c, mine, other):
+    def project_pair(block, c, mine, other, layers=(0, 1)):
         lines = jnp.concatenate([src[mine, c], src[other, c]], axis=0)
-        project(lines, block, c * 2 * chunk)
+        place = pl.ds(c * 2 * chunk, 2 * chunk)
+        if 0 in layers:
+            first = dot(lines, keyval_first[...])
+            k_first[block, place] = first[:, :HEAD].astype(BF16)
+            v_first[block, place] = first[:, HEAD:].astype(BF16)
+        if 1 in layers:
+            second = dot(lines, keyval_second[...])
+            k_second[z, block, place] = second[:, :HEAD].astype(BF16)
+            v_second[z, block, place] = second[:, HEAD:].astype(BF16)
 
     def absorb(keys, values, queries, slot, fresh):
         scores = dot(keys, queries)
@@ -365,24 +385,36 @@
     for d in range(1, n_sp):
         q_copy(d, sp_at(d)).wait_recv()
     kv_hop(0, 1, arrive=False)
-    absorb_block(0, True)
-
-    def far_chip(d):
+    with SC("abs_own"):
+        absorb_block(0, True)
+
+    def far_chunk(d, c, layers=(0, 1)):
         near = tp_at(2 * d)
         far = lax.rem(sib + 2 * d, n_tp)
+        src_copy(near, c, sib, 1).wait_recv()
+        src_copy(near, c, sib, 1).start()
+        src_copy(far, c, sib, 1).wait_recv()
+        project_pair(d, c, near, far, layers)
+
+    def far_absorb(d):
         for c in range(CHUNKS):
-            src_copy(near, c, sib, 1).wait_recv()
-            src_copy(near, c, sib, 1).start()
-            src_copy(far, c, sib, 1).wait_recv()
-            project_pair(d, c, near, far)
-
-    def far_absorb(d):
-        far_chip(d)
+            far_chunk(d, c)
         absorb_block(d, False)
 
     times(1, n_chip - 1, far_absorb)
     last = n_chip - 1
-    far_chip(last)
+    early = (CHUNKS - 1) * 2 * chunk
+    with SC("far_early"):
+        for c in range(CHUNKS - 1):
+            far_chunk(last, c)
+
+    with SC("abs_early"):
+        @pl.loop(0, n_sp)
+        def _(slot):
+            absorb(k_first[last, :early], v_first[last, :early], q_slots[slot], slot, False)
+
+    with SC("far_last"):
+        far_chunk(last, CHUNKS - 1, (0,))
 
     def mix_copies(distance, slot):
         peer = sp_at(distance)
@@ -392,7 +424,7 @@
         ]
 
     def finish_slot(slot, mixes, stats):
-        absorb(k_first[last], v_first[last], q_slots[slot], slot, False)
+        absorb(k_first[last, early:], v_first[last, early:], q_slots[slot], slot, False)
         total = run_sum[slot]
         mixes[slot] = (run_out[slot] / total).astype(BF16)
         stats[slot] = jnp.concatenate([run_max[slot], total], axis=0)
@@ -403,13 +435,27 @@
         for copy in mix_copies(d, z):
             copy.start()
 
-    finish_slot(z, mix_recv, stat_recv)
-    for d in range(1, n_sp):
-        for copy in mix_copies(d, sp_at(d)):
-            copy.wait_recv()
-    kv_hop(0, 2)
-    for block in range(1, n_chip):
-        kv_hop(block, 1, arrive=False)
+    with SC("finish_me"):
+        finish_slot(z, mix_recv, stat_recv)
+        project_pair(last, CHUNKS - 1, tp_at(2 * last), lax.rem(sib + 2 * last, n_tp), (1,))
+    with SC("transpose"):
+        loads[6].wait()
+        loads[7].wait()
+        stripe = 2 * HEAD
+
+        @pl.loop(0, width // stripe)
+        def _(index):
+            place = pl.ds(pl.multiple_of(index * stripe, stripe), stripe)
+            w_gate[place, :] = gate_t[:, place].T
+            w_value[place, :] = value_t[:, place].T
+
+    with SC("mixwait"):
+        for d in range(1, n_sp):
+            for copy in mix_copies(d, sp_at(d)):
+                copy.wait_recv()
+    with SC("kv_a"):
+        for block in range(1, n_chip):
+            kv_hop(block, 1, arrive=False)
     top = stat_recv[0, 0:1]
     for slot in range(1, n_sp):
         top = jnp.maximum(top, stat_recv[slot, 0:1])
@@ -420,73 +466,97 @@
         weight_sum = weight_sum + share
         weighted = weighted + mix_recv[slot].astype(F32) * share
     loads[5].wait()
-    mixed = scatter_sum(0, head_rows(weighted / weight_sum), out_first)
+    with SC("rs0"):
+        mixed = scatter_sum(0, head_rows(weighted / weight_sum), out_first)
     after_first = target_v[...].astype(F32) + normed(mixed, post_first[...])
     stream[...] = after_first
 
-    gather_start(1, normed(after_first, ffn_pre[...]))
-    kv_hop(0, 3)
-    for block in range(1, n_chip):
-        kv_hop(block, 2)
-    loads[6].wait()
-    loads[7].wait()
-    up_gate, up_value = (up.astype(BF16) for up in gather_times(1, [w_gate, w_value]))
-    halo_send[0] = up_gate[block_rows - 16 :]
-    halo_send[1] = up_value[block_rows - 16 :]
-    halo = to_sp(halo_send, halo_recv, halo_sem.at[0], halo_sem.at[1], sp_at(1))
-
-    @pl.when(z < n_sp - 1)
+    def halo_copy(device):
+        return pltpu.make_async_remote_copy(
+            src_ref=halo_send, dst_ref=halo_recv, send_sem=halo_sem.at[0],
+            recv_sem=halo_sem.at[1], device_id=device, device_id_type=MESH,
+        )
+
+    ffn_input = normed(after_first, ffn_pre[...])
+
+    @pl.when(gives_halo)
     def _():
-        halo.start()
-
-    @pl.when(z > 0)
-    def _():
-        halo.wait_recv()
-
-    def causal_mix(up_rows, rim, taps):
-        here = up_rows.astype(F32)
-        rim = jnp.where(z > 0, rim.astype(F32), 0.0)
+        halo_send[...] = ffn_input[rows - 2 :].astype(BF16)
+        for t in range(n_tp):
+            halo_copy({"sp": z + 1, "tp": t}).start()
+
+    gather_start(1, ffn_input)
+    with SC("kv_b"):
+        kv_hop(0, 2)
+
+    def halo_rows():
+        @pl.when(z > 0)
+        def _():
+            halo_copy({"sp": z, "tp": sib}).wait_recv()
+
+        zeros = jnp.zeros((14, width), F32)
+        return jnp.concatenate([halo_recv[...].astype(F32), zeros], axis=0).astype(BF16)
+
+    with SC("ag1_up"):
+        up_gate, up_value = (
+            up.astype(BF16) for up in gather_times(1, [w_gate, w_value], halo_rows)
+        )
+
+    def causal_mix(up_rows, taps):
+        here = up_rows[:block_rows].astype(F32)
+        rim = jnp.where(z > 0, up_rows[block_rows:].astype(F32), 0.0)
         row = lax.broadcasted_iota(jnp.int32, here.shape, 0)
-        before = jnp.where(row == 0, rim[15:16], pltpu.roll(here, 1, 0))
+        before = jnp.where(row == 0, rim[1:2], pltpu.roll(here, 1, 0))
         earlier = jnp.where(
-            row == 0, rim[14:15], jnp.where(row == 1, rim[15:16], pltpu.roll(here, 2, 0))
+            row == 0, rim[0:1], jnp.where(row == 1, rim[1:2], pltpu.roll(here, 2, 0))
         )
         return taps[0:1] * earlier + taps[1:2] * before + taps[2:3] * here
 
-    gated = (
-        jax.nn.gelu(causal_mix(up_gate, halo_recv[0], conv_gate[...]), approximate=True)
-        * causal_mix(up_value, halo_recv[1], conv_value[...])
-    ).astype(BF16)
-    loads[8].wait()
-    ffn_sum = scatter_sum(1, gated, w_down)
+    with SC("gated"):
+        gated = (
+            jax.nn.gelu(causal_mix(up_gate, conv_gate[...]), approximate=True)
+            * causal_mix(up_value, conv_value[...])
+        ).astype(BF16)
+        loads[8].wait()
+    with SC("kv_c"):
+        for block in range(1, n_chip):
+            kv_hop(block, 2)
+    with SC("rs1"):
+        ffn_sum = scatter_sum(1, gated, w_down)
     after_ffn = stream[...] + normed(ffn_sum, ffn_post[...])
     stream[...] = after_ffn
 
     gather_start(2, normed(after_ffn, pre_second[...]))
-    for block in range(1, n_chip):
-        kv_hop(block, 3)
-    loads[9].wait()
-    queries = head_columns(gather_times(2, [query_second])[0])
-    for d in range(1, n_sp):
-        q_copy(d, None).wait_send()
-    q_slots[z] = queries
-
-    for block in range(n_chip):
-        absorb(k_second[z, block], v_second[z, block], q_slots[z], 0, block == 0)
-
-    @pl.loop(4, max(n_sp, 4) + 1)
-    def _(hop):
+    with SC("kv_d"):
         for block in range(n_chip):
-            kv_hop(block, hop)
-
-    @pl.loop(1, n_sp)
-    def _(d):
-        slot = sp_at(d)
+            kv_hop(block, 3)
+    with SC("ag2_q"):
+        loads[9].wait()
+        queries = head_columns(gather_times(2, [query_second])[0])
+        for d in range(1, n_sp):
+            q_copy(d, None).wait_send()
+        q_slots[z] = queries
+
+    with SC("attn2_own"):
         for block in range(n_chip):
-            absorb(k_second[slot, block], v_second[slot, block], q_slots[z], 0, False)
-
-    loads[10].wait()
-    mixed = scatter_sum(2, head_rows(run_out[0] / run_sum[0]), out_second)
+            absorb(k_second[z, block], v_second[z, block], q_slots[z], 0, block == 0)
+
+    with SC("kv_e"):
+        @pl.loop(4, max(n_sp, 4) + 1)
+        def _(hop):
+            for block in range(n_chip):
+                kv_hop(block, hop)
+
+    with SC("attn2_rest"):
+        @pl.loop(1, n_sp)
+        def _(d):
+            slot = sp_at(d)
+            for block in range(n_chip):
+                absorb(k_second[slot, block], v_second[slot, block], q_slots[z], 0, False)
+
+    with SC("rs2"):
+        loads[10].wait()
+        mixed = scatter_sum(2, head_rows(run_out[0] / run_sum[0]), out_second)
     decoded[...] = stream[...] + normed(mixed, post_second[...])
 
     for phase in range(3):
@@ -506,9 +576,10 @@
 
     times(1, n_sp, drain)
 
-    @pl.when(z < n_sp - 1)
+    @pl.when(gives_halo)
     def _():
-        halo.wait_send()
+        for t in range(n_tp):
+            halo_copy({"sp": z, "tp": sib}).wait_send()
 
 
 def per_device(*arrays):
@@ -527,7 +598,6 @@
     lines = source.shape[0]
     block_rows = rows * n_tp
     columns = query_first.shape[1] // HEAD * block_rows
-    hidden_units = w_gate.shape[1]
     n_chip = n_tp // 2
     span = width // PIECES
     dma = pltpu.SemaphoreType.DMA
@@ -541,7 +611,7 @@
         pltpu.VMEM(target.shape, BF16),
         pltpu.VMEM(source.shape, BF16),
         *(pltpu.VMEM(w.shape, BF16) for w in (
-            query_first, keyval_first, out_first, w_gate, w_value, w_down,
+            query_first, keyval_first, out_first, w_gate.T, w_value.T, w_gate, w_value, w_down,
             query_second, keyval_second, out_second)),
         dma((11,)),
         pltpu.VMEM((3, PIECES, n_tp, rows, span), BF16),
@@ -573,8 +643,8 @@
         dma((3, 2)),
         dma((3, PIECES)),
         dma((3, PIECES, n_chip)),
-        pltpu.VMEM((2, 16, hidden_units), BF16),
-        pltpu.VMEM((2, 16, hidden_units), BF16),
+        pltpu.VMEM((2, width), BF16),
+        pltpu.VMEM((2, width), BF16),
         dma((2,)),
         pltpu.VMEM((rows, width), F32),
     ]
@@ -596,7 +666,7 @@
         name="decoder",
     )(
         target, source, row(source_gain), row(pre_first), query_first, keyval_first, out_first,
-        row(post_first), row(ffn_pre), w_gate, w_value, conv_gate, conv_value, w_down,
+        row(post_first), row(ffn_pre), w_gate.T, w_value.T, conv_gate, conv_value, w_down,
         row(ffn_post), row(pre_second), query_second, keyval_second, out_second, row(post_second),
     )
 

time: 105 us -> 94.8 us (0.903)
  the two profiles are of different devices: /device:TPU:30 before, /device:TPU:0 now
where the time goes in v1:
time: 94.8 us; the launch traced here: 94.6 us
  Pallas kernels  92.9 us (98%)
  local copies, waits for them, and re-layouts  1.67 us (2%)
    pallas_call x1, Pallas kernels, per_device(): pl.pallas_call(kernel, out_shape=jax.ShapeDtypeStruct((rows, width), F32)...  92.9 us

profile of v1, /device:TPU:0, one launch (start us, length us, event | category | flops | bytes accessed | tf_op | source)
XLA Modules:
  0.0 94.6 jit_solution(6229506133902522111)
XLA Ops:
  0.0 92.9 %decoder.1 = f32[32,2048]{1,0:T(8,128)} custom-call(bf16[32,2048]{1,0:T(8,128)(2,1)} %refs_0_.1, bf16[256,2048]{1,0:T(8,128)(2,1)} %refs_1_.1, f32[1,2048]{1,0:T(1,128)} %bitcast.11, f32[1,2048]{1,0:T(1,128)} %bitcast.12, bf16[2048,512]{1,0:T(8,128)(2,1)} %refs_4_.1, bf16[2048,256]{1,0:T(8,128)(2,1)} %refs_5_.1, bf16[512,2048]{1,0:T(8,128)(2,1)} %refs_6_.1, ...), custom_call_target="tpu_custom_call" | custom-call | tf_op jit(solution)/shard_map/decoder/pallas_call | solution.py:655
  92.9 1.7 %copy.22 = f32[32,2048]{1,0:T(8,128)} copy(f32[32,2048]{1,0:T(8,128)} %decoder.1) | data formatting | bytes 524288

commit v2 on v1

--- a/solution.py
+++ b/solution.py
@@ -43,25 +43,35 @@
     n_sp,
     target_h,
     source_h,
-    source_gain,
-    pre_first,
+    source_gain_h,
+    pre_first_h,
     query_first_h,
     keyval_first_h,
     out_first_h,
-    post_first,
-    ffn_pre,
+    post_first_h,
+    ffn_pre_h,
     gate_h,
     value_h,
-    conv_gate,
-    conv_value,
+    conv_gate_h,
+    conv_value_h,
     down_h,
-    ffn_post,
-    pre_second,
+    ffn_post_h,
+    pre_second_h,
     query_second_h,
     keyval_second_h,
     out_second_h,
+    post_second_h,
+    decoded,
+    source_gain,
+    pre_first,
+    post_first,
+    ffn_pre,
+    conv_gate,
+    conv_value,
+    ffn_post,
+    pre_second,
     post_second,
-    decoded,
+    vec_sem,
     target_v,
     source_v,
     query_first,
@@ -86,8 +96,7 @@
     q_sem,
     k_first,
     v_first,
-    k_second,
-    v_second,
+    kv_second,
     kv_send,
     kv_recv,
     run_max,
@@ -155,8 +164,27 @@
     loads = [
         pltpu.make_async_copy(a, b, local_sem.at[i]) for i, (a, b) in enumerate(pairs)
     ]
-    for load in loads:
+    vectors = {
+        name: pltpu.make_async_copy(a, b, vec_sem.at[i])
+        for i, (name, a, b) in enumerate([
+            ("pre_first", pre_first_h, pre_first),
+            ("source_gain", source_gain_h, source_gain),
+            ("post_first", post_first_h, post_first),
+            ("ffn_pre", ffn_pre_h, ffn_pre),
+            ("conv_gate", conv_gate_h, conv_gate),
+            ("conv_value", conv_value_h, conv_value),
+            ("ffn_post", ffn_post_h, ffn_post),
+            ("pre_second", pre_second_h, pre_second),
+            ("post_second", post_second_h, post_second),
+        ])
+    }
+    loads[0].start()
+    vectors["pre_first"].start()
+    vectors["source_gain"].start()
+    for load in loads[1:]:
         load.start()
+    for name in list(vectors)[2:]:
+        vectors[name].start()
 
     barrier = pltpu.get_barrier_semaphore()
     for distance in range(1, n_tp):
@@ -276,6 +304,7 @@
         return jnp.concatenate(blocks, axis=1).astype(BF16)
 
     loads[0].wait()
+    vectors["pre_first"].wait()
     with SC("norm0"):
         gather_start(0, normed(target_v[...], pre_first[...]))
 
@@ -285,6 +314,7 @@
         )
 
     loads[1].wait()
+    vectors["source_gain"].wait()
     for c in range(CHUNKS):
         src[me, c] = normed(source_v[pl.ds(c * chunk, chunk)], source_gain[...]).astype(BF16)
         for d in range(1, n_chip):
@@ -316,8 +346,8 @@
             v_first[block, place] = first[:, HEAD:].astype(BF16)
         if 1 in layers:
             second = dot(lines, keyval_second[...])
-            k_second[z, block, place] = second[:, :HEAD].astype(BF16)
-            v_second[z, block, place] = second[:, HEAD:].astype(BF16)
+            kv_second[z, block, c, 0] = second[:, :HEAD].astype(BF16)
+            kv_second[z, block, c, 1] = second[:, HEAD:].astype(BF16)
 
     def absorb(keys, values, queries, slot, fresh):
         scores = dot(keys, queries)
@@ -342,16 +372,11 @@
         def _(slot):
             absorb(k_first[block], v_first[block], q_slots[slot], slot, fresh)
 
-    def kv_copies(block, slot, peer):
-        return [
-            to_sp(
-                store.at[slot, block], store.at[slot, block],
-                kv_send.at[index], kv_recv.at[index, slot, block], peer,
-            )
-            for index, store in enumerate((k_second, v_second))
-        ]
-
-    def kv_hop(block, hop, arrive=True, leave=True):
+    def kv_copy(block, slot, c, peer):
+        held = kv_second.at[slot, block, c]
+        return to_sp(held, held, kv_send, kv_recv.at[slot, block, c], peer)
+
+    def kv_hop(block, hop, arrive=True, chunks=range(CHUNKS)):
         for step in (1, -1):
             slot = z - step * (hop - 1)
             peer = z + step
@@ -359,14 +384,13 @@
             @pl.when(jnp.logical_and(slot >= 0, slot < n_sp))
             def _():
                 if arrive:
-                    for copy in kv_copies(block, slot, sp_at(1)):
-                        copy.wait_recv()
-                if leave:
-
-                    @pl.when(jnp.logical_and(hop < n_sp, jnp.logical_and(peer >= 0, peer < n_sp)))
-                    def _():
-                        for copy in kv_copies(block, slot, peer):
-                            copy.start()
+                    for c in chunks:
+                        kv_copy(block, slot, c, sp_at(1)).wait_recv()
+
+                @pl.when(jnp.logical_and(hop < n_sp, jnp.logical_and(peer >= 0, peer < n_sp)))
+                def _():
+                    for c in chunks:
+                        kv_copy(block, slot, c, peer).start()
 
     def kv_drain(block, hop):
         for step in (1, -1):
@@ -376,8 +400,17 @@
 
             @pl.when(jnp.logical_and(inside, jnp.logical_and(peer >= 0, peer < n_sp)))
             def _():
-                for copy in kv_copies(block, slot, peer):
-                    copy.wait_send()
+                for c in range(CHUNKS):
+                    kv_copy(block, slot, c, peer).wait_send()
+
+    def nearest(j):
+        up = j + jnp.where(j >= z, 1, 0)
+        down = n_sp - 1 - j
+        down = down - jnp.where(down <= z, 1, 0)
+        return jnp.where(2 * z < n_sp, up, down)
+
+    def second_rows(slot, part):
+        return kv_second[slot, :, :, part].reshape(n_chip * CHUNKS * 2 * chunk, HEAD)
 
     for c in range(CHUNKS):
         src_copy(sib, c, sib, 0).wait_recv()
@@ -407,6 +440,8 @@
     with SC("far_early"):
         for c in range(CHUNKS - 1):
             far_chunk(last, c)
+            if n_chip > 1:
+                kv_hop(last, 1, False, (c,))
 
     with SC("abs_early"):
         @pl.loop(0, n_sp)
@@ -416,8 +451,7 @@
     with SC("far_last"):
         far_chunk(last, CHUNKS - 1, (0,))
 
-    def mix_copies(distance, slot):
-        peer = sp_at(distance)
+    def mix_copies(peer, slot):
         return [
             to_sp(sent.at[peer], got.at[slot], mix_sem.at[index, 0, 0], mix_sem.at[index, 1, slot], peer)
             for index, (sent, got) in enumerate(((mix_send, mix_recv), (stat_send, stat_recv)))
@@ -429,10 +463,11 @@
         mixes[slot] = (run_out[slot] / total).astype(BF16)
         stats[slot] = jnp.concatenate([run_max[slot], total], axis=0)
 
-    @pl.loop(1, n_sp)
-    def _(d):
-        finish_slot(sp_at(d), mix_send, stat_send)
-        for copy in mix_copies(d, z):
+    @pl.loop(0, n_sp - 1)
+    def _(j):
+        peer = nearest(n_sp - 2 - j)
+        finish_slot(peer, mix_send, stat_send)
+        for copy in mix_copies(peer, z):
             copy.start()
 
     with SC("finish_me"):
@@ -441,6 +476,8 @@
     with SC("transpose"):
         loads[6].wait()
         loads[7].wait()
+        for name in list(vectors)[2:]:
+            vectors[name].wait()
         stripe = 2 * HEAD
 
         @pl.loop(0, width // stripe)
@@ -451,11 +488,13 @@
 
     with SC("mixwait"):
         for d in range(1, n_sp):
-            for copy in mix_copies(d, sp_at(d)):
+            for copy in mix_copies(sp_at(d), sp_at(d)):
                 copy.wait_recv()
     with SC("kv_a"):
-        for block in range(1, n_chip):
-            kv_hop(block, 1, arrive=False)
+        kv_hop(last, 1, False, (CHUNKS - 1,))
+        for block in range(1, last):
+            kv_hop(block, 1, False)
+        kv_hop(0, 2)
     top = stat_recv[0, 0:1]
     for slot in range(1, n_sp):
         top = jnp.maximum(top, stat_recv[slot, 0:1])
@@ -487,7 +526,8 @@
 
     gather_start(1, ffn_input)
     with SC("kv_b"):
-        kv_hop(0, 2)
+        for block in range(1, n_chip):
+            kv_hop(block, 2)
 
     def halo_rows():
         @pl.when(z > 0)
@@ -519,8 +559,7 @@
         ).astype(BF16)
         loads[8].wait()
     with SC("kv_c"):
-        for block in range(1, n_chip):
-            kv_hop(block, 2)
+        kv_hop(0, 3)
     with SC("rs1"):
         ffn_sum = scatter_sum(1, gated, w_down)
     after_ffn = stream[...] + normed(ffn_sum, ffn_post[...])
@@ -528,7 +567,7 @@
 
     gather_start(2, normed(after_ffn, pre_second[...]))
     with SC("kv_d"):
-        for block in range(n_chip):
+        for block in range(1, n_chip):
             kv_hop(block, 3)
     with SC("ag2_q"):
         loads[9].wait()
@@ -538,21 +577,27 @@
         q_slots[z] = queries
 
     with SC("attn2_own"):
-        for block in range(n_chip):
-            absorb(k_second[z, block], v_second[z, block], q_slots[z], 0, block == 0)
-
-    with SC("kv_e"):
+        absorb(second_rows(z, 0), second_rows(z, 1), q_slots[z], 0, True)
+
+    def kv_rest():
         @pl.loop(4, max(n_sp, 4) + 1)
         def _(hop):
             for block in range(n_chip):
                 kv_hop(block, hop)
 
+    def absorb_second(j):
+        slot = nearest(j)
+        absorb(second_rows(slot, 0), second_rows(slot, 1), q_slots[z], 0, False)
+
     with SC("attn2_rest"):
-        @pl.loop(1, n_sp)
-        def _(d):
-            slot = sp_at(d)
-            for block in range(n_chip):
-                absorb(k_second[slot, block], v_second[slot, block], q_slots[z], 0, False)
+        if n_sp > 4:
+            kv_rest()
+        times(0, n_sp - 2, absorb_second)
+    with SC("kv_e"):
+        if n_sp <= 4:
+            kv_rest()
+    with SC("attn2_last"):
+        absorb_second(n_sp - 2)
 
     with SC("rs2"):
         loads[10].wait()
@@ -571,7 +616,7 @@
     def drain(d):
         for block in range(n_chip):
             kv_drain(block, d)
-        for copy in mix_copies(d, z):
+        for copy in mix_copies(sp_at(d), z):
             copy.wait_send()
 
     times(1, n_sp, drain)
@@ -601,13 +646,16 @@
     n_chip = n_tp // 2
     span = width // PIECES
     dma = pltpu.SemaphoreType.DMA
-    any_spec = pl.BlockSpec(memory_space=pl.ANY)
+    hbm = pl.BlockSpec(memory_space=pltpu.HBM)
     vmem = pl.BlockSpec(memory_space=pltpu.VMEM)
 
     def row(gain):
         return gain.reshape(1, width)
 
+    line = pltpu.VMEM((1, width), F32)
     scratch = [
+        *([line] * 4), pltpu.VMEM(conv_gate.shape, F32), pltpu.VMEM(conv_value.shape, F32),
+        *([line] * 3), dma((9,)),
         pltpu.VMEM(target.shape, BF16),
         pltpu.VMEM(source.shape, BF16),
         *(pltpu.VMEM(w.shape, BF16) for w in (
@@ -624,10 +672,9 @@
         dma((2, n_sp)),
         pltpu.VMEM((n_chip, 2 * lines, HEAD), BF16),
         pltpu.VMEM((n_chip, 2 * lines, HEAD), BF16),
-        pltpu.VMEM((n_sp, n_chip, 2 * lines, HEAD), BF16),
-        pltpu.VMEM((n_sp, n_chip, 2 * lines, HEAD), BF16),
-        dma((2,)),
-        dma((2, n_sp, n_chip)),
+        pltpu.VMEM((n_sp, n_chip, CHUNKS, 2, 2 * lines // CHUNKS, HEAD), BF16),
+        dma,
+        dma((n_sp, n_chip, CHUNKS)),
         pltpu.VMEM((n_sp, 1, columns), F32),
         pltpu.VMEM((n_sp, 1, columns), F32),
         pltpu.VMEM((n_sp, HEAD, columns), F32),
@@ -654,14 +701,12 @@
 
     return pl.pallas_call(
         kernel,
-        out_shape=jax.ShapeDtypeStruct((rows, width), F32),
-        in_specs=[any_spec, any_spec, vmem, vmem, any_spec, any_spec, any_spec, vmem, vmem,
-                  any_spec, any_spec, vmem, vmem, any_spec, vmem, vmem, any_spec, any_spec,
-                  any_spec, vmem],
+        out_shape=pltpu.VMEM((rows, width), F32),
+        in_specs=[hbm] * 20,
         out_specs=vmem,
         scratch_shapes=scratch,
         compiler_params=pltpu.CompilerParams(
-            collective_id=0, has_side_effects=True, vmem_limit_bytes=67_000_000
+            collective_id=0, has_side_effects=True, vmem_limit_bytes=60_000_000
         ),
         name="decoder",
     )(

time: 94.8 us -> 84.1 us (0.89)
  Pallas kernels: 92.9 us -> 83.2 us
  local copies, waits for them, and re-layouts: 1.67 us -> 0.71 us
    pallas_call x1, Pallas kernels: 92.9 us -> 83.2 us  [per_device(): pl.pallas_call(kernel, out_shape=pltpu.VMEM((rows, width), F32), in_specs...]
    unnamed x1, local copies, waits for them, and re-layouts: 1.67 us -> 0.71 us
where the time goes in v2:
time: 84.1 us; the launch traced here: 83.9 us
  Pallas kernels  83.2 us (99%)
    pallas_call x1, Pallas kernels, per_device(): pl.pallas_call(kernel, out_shape=pltpu.VMEM((rows, width), F32), in_specs...  83.2 us

profile of v2, /device:TPU:0, one launch (start us, length us, event | category | flops | bytes accessed | tf_op | source)
XLA Modules:
  0.0 83.9 jit_solution(11775698333359550922)
XLA Ops:
  0.0 83.2 %decoder.1 = f32[32,2048]{1,0:T(8,128)S(1)} custom-call(bf16[32,2048]{1,0:T(8,128)(2,1)} %refs_0_.1, bf16[256,2048]{1,0:T(8,128)(2,1)} %refs_1_.1, f32[1,2048]{1,0:T(1,128)} %bitcast.11, f32[1,2048]{1,0:T(1,128)} %bitcast.12, bf16[2048,512]{1,0:T(8,128)(2,1)} %refs_4_.1, bf16[2048,256]{1,0:T(8,128)(2,1)} %refs_5_.1, bf16[512,2048]{1,0:T(8,128)(2,1)} %refs_6_.1, ...), custom_call_target="tpu_custom_call" | custom-call | tf_op jit(solution)/shard_map/decoder/pallas_call | solution.py:702
  83.2 0.7 copy.22

commit v3 on v2

--- a/solution.py
+++ b/solution.py
@@ -118,6 +118,9 @@
     halo_recv,
     halo_sem,
     stream,
+    relay_mix,
+    relay_stat,
+    relay_sem,
 ):
     me = lax.axis_index("tp")
     z = lax.axis_index("sp")
@@ -321,22 +324,6 @@
             src_copy(me, c, tp_at(2 * d), 0).start()
         src_copy(me, c, sib, 0).start()
 
-    loads[2].wait()
-    with SC("qproj"):
-        q_slots[z] = head_columns(gather_times(0, [query_first])[0])
-
-    def q_copy(distance, slot):
-        return to_sp(
-            q_slots.at[z], q_slots.at[z] if slot is None else q_slots.at[slot],
-            q_sem.at[0, 0], q_sem.at[1, z if slot is None else slot], sp_at(distance),
-        )
-
-    for d in range(1, n_sp):
-        q_copy(d, None).start()
-
-    loads[3].wait()
-    loads[4].wait()
-
     def project_pair(block, c, mine, other, layers=(0, 1)):
         lines = jnp.concatenate([src[mine, c], src[other, c]], axis=0)
         place = pl.ds(c * 2 * chunk, 2 * chunk)
@@ -350,7 +337,9 @@
             kv_second[z, block, c, 1] = second[:, HEAD:].astype(BF16)
 
     def absorb(keys, values, queries, slot, fresh):
-        scores = dot(keys, queries)
+        absorb_scores(dot(keys, queries), values, slot, fresh)
+
+    def absorb_scores(scores, values, slot, fresh):
         newest = jnp.max(scores, axis=0, keepdims=True)
         if not fresh:
             newest = jnp.maximum(newest, run_max[slot])
@@ -412,44 +401,87 @@
     def second_rows(slot, part):
         return kv_second[slot, :, :, part].reshape(n_chip * CHUNKS * 2 * chunk, HEAD)
 
-    for c in range(CHUNKS):
-        src_copy(sib, c, sib, 0).wait_recv()
-        project_pair(0, c, me, sib)
+    loads[3].wait()
+    loads[4].wait()
+    with SC("proj_own"):
+        for c in range(CHUNKS):
+            src_copy(sib, c, sib, 0).wait_recv()
+            project_pair(0, c, me, sib)
+    kv_hop(0, 1, False, range(CHUNKS // 2))
+    loads[2].wait()
+    with SC("qproj"):
+        q_slots[z] = head_columns(gather_times(0, [query_first])[0])
+
+    def q_copy(distance, slot):
+        return to_sp(
+            q_slots.at[z], q_slots.at[z] if slot is None else q_slots.at[slot],
+            q_sem.at[0, 0], q_sem.at[1, z if slot is None else slot], sp_at(distance),
+        )
+
     for d in range(1, n_sp):
-        q_copy(d, sp_at(d)).wait_recv()
-    kv_hop(0, 1, arrive=False)
+        q_copy(d, None).start()
+
+    last = n_chip - 1
+    lead = CHUNKS // 2
+
+    def near_chunk(d, c):
+        near = tp_at(2 * d)
+        src_copy(near, c, sib, 1).wait_recv()
+        src_copy(near, c, sib, 1).start()
+
+    def far_chunk(d, c, layers=(0, 1)):
+        far = lax.rem(sib + 2 * d, n_tp)
+        src_copy(far, c, sib, 1).wait_recv()
+        project_pair(d, c, tp_at(2 * d), far, layers)
+
+    def absorb_chunks(low, high):
+        place = slice(low * 2 * chunk, high * 2 * chunk)
+
+        @pl.loop(0, n_sp)
+        def _(slot):
+            absorb(k_first[last, place], v_first[last, place], q_slots[slot], slot, False)
+
+    def lead_chunks():
+        for c in range(lead):
+            near_chunk(last, c)
+            far_chunk(last, c)
+
+    if n_chip == 2:
+        with SC("lead"):
+            lead_chunks()
+    with SC("qwait"):
+        for d in range(1, n_sp):
+            q_copy(d, sp_at(d)).wait_recv()
+    kv_hop(0, 1, False, range(lead, CHUNKS))
+    kv_hop(0, 2, True, range(lead))
     with SC("abs_own"):
         absorb_block(0, True)
 
-    def far_chunk(d, c, layers=(0, 1)):
-        near = tp_at(2 * d)
-        far = lax.rem(sib + 2 * d, n_tp)
-        src_copy(near, c, sib, 1).wait_recv()
-        src_copy(near, c, sib, 1).start()
-        src_copy(far, c, sib, 1).wait_recv()
-        project_pair(d, c, near, far, layers)
-
     def far_absorb(d):
         for c in range(CHUNKS):
+            near_chunk(d, c)
             far_chunk(d, c)
         absorb_block(d, False)
 
-    times(1, n_chip - 1, far_absorb)
-    last = n_chip - 1
-    early = (CHUNKS - 1) * 2 * chunk
-    with SC("far_early"):
-        for c in range(CHUNKS - 1):
+    times(1, last, far_absorb)
+    if n_chip > 2:
+        lead_chunks()
+    kv_hop(last, 1, False, range(lead))
+    for c in range(lead, CHUNKS - 1):
+        with SC("near"):
+            near_chunk(last, c)
+        with SC("abs_early"):
+            absorb_chunks(0 if c == lead else c - 1, c)
+        with SC("far"):
             far_chunk(last, c)
-            if n_chip > 1:
-                kv_hop(last, 1, False, (c,))
-
-    with SC("abs_early"):
-        @pl.loop(0, n_sp)
-        def _(slot):
-            absorb(k_first[last, :early], v_first[last, :early], q_slots[slot], slot, False)
-
+        kv_hop(last, 1, False, (c,))
+    with SC("abs_early2"):
+        absorb_chunks(CHUNKS - 2, CHUNKS - 1)
+    with SC("near_last"):
+        near_chunk(last, CHUNKS - 1)
     with SC("far_last"):
         far_chunk(last, CHUNKS - 1, (0,))
+    early = (CHUNKS - 1) * 2 * chunk
 
     def mix_copies(peer, slot):
         return [
@@ -457,21 +489,64 @@
             for index, (sent, got) in enumerate(((mix_send, mix_recv), (stat_send, stat_recv)))
         ]
 
-    def finish_slot(slot, mixes, stats):
+    def finish_slot(slot):
         absorb(k_first[last, early:], v_first[last, early:], q_slots[slot], slot, False)
-        total = run_sum[slot]
-        mixes[slot] = (run_out[slot] / total).astype(BF16)
-        stats[slot] = jnp.concatenate([run_max[slot], total], axis=0)
-
-    @pl.loop(0, n_sp - 1)
-    def _(j):
-        peer = nearest(n_sp - 2 - j)
-        finish_slot(peer, mix_send, stat_send)
+
+    def pack(peer):
+        total = run_sum[peer]
+        mix_send[peer] = (run_out[peer] / total).astype(BF16)
+        stat_send[peer] = jnp.concatenate([run_max[peer], total], axis=0)
+
+    def finish_and_send(peer):
+        finish_slot(peer)
+        pack(peer)
         for copy in mix_copies(peer, z):
             copy.start()
 
+    relayed = n_sp > 2
+    end = n_sp - 1
+    gives, merges, takes = z == 0, z == 1, z == end
+
+    def relay_copies():
+        return [
+            to_sp(sent.at[end], got, relay_sem.at[index, 0], relay_sem.at[index, 1], 1)
+            for index, (sent, got) in enumerate(((mix_send, relay_mix), (stat_send, relay_stat)))
+        ]
+
+    def mix_order(j):
+        return jnp.where(
+            merges, jnp.where(j == n_sp - 2, end, nearest(n_sp - 2 - j - 1)), nearest(n_sp - 2 - j)
+        )
+
+    if relayed:
+
+        @pl.loop(0, n_sp - 1)
+        def _(j):
+            peer = mix_order(j)
+            finish_slot(peer)
+
+            @pl.when(jnp.logical_not(jnp.logical_and(merges, peer == end)))
+            def _():
+                pack(peer)
+
+                @pl.when(jnp.logical_and(gives, peer == end))
+                def _():
+                    for copy in relay_copies():
+                        copy.start()
+
+                @pl.when(jnp.logical_not(jnp.logical_and(gives, peer == end)))
+                def _():
+                    for copy in mix_copies(peer, z):
+                        copy.start()
+
+    else:
+
+        @pl.loop(0, n_sp - 1)
+        def _(j):
+            finish_and_send(nearest(n_sp - 2 - j))
+
     with SC("finish_me"):
-        finish_slot(z, mix_recv, stat_recv)
+        finish_slot(z)
         project_pair(last, CHUNKS - 1, tp_at(2 * last), lax.rem(sib + 2 * last, n_tp), (1,))
     with SC("transpose"):
         loads[6].wait()
@@ -486,27 +561,49 @@
             w_gate[place, :] = gate_t[:, place].T
             w_value[place, :] = value_t[:, place].T
 
+    def merge_into(slot, values, newest, count):
+        top = jnp.maximum(newest, run_max[slot])
+        rescale = jnp.exp2((run_max[slot] - top) * EXP_SCALE)
+        share = jnp.exp2((newest - top) * EXP_SCALE) * count
+        run_max[slot] = top
+        run_sum[slot] = run_sum[slot] * rescale + share
+        run_out[slot] = run_out[slot] * rescale + values.astype(F32) * share
+
+    def merge(slot):
+        for copy in mix_copies(slot, slot):
+            copy.wait_recv()
+        merge_into(z, mix_recv[slot], stat_recv[slot, 0:1], stat_recv[slot, 1:2])
+
+    if relayed:
+        with SC("relay"):
+
+            @pl.when(merges)
+            def _():
+                for copy in relay_copies():
+                    copy.wait_recv()
+                merge_into(end, relay_mix[...], relay_stat[0:1], relay_stat[1:2])
+                pack(end)
+                for copy in mix_copies(end, z):
+                    copy.start()
+
     with SC("mixwait"):
-        for d in range(1, n_sp):
-            for copy in mix_copies(sp_at(d), sp_at(d)):
-                copy.wait_recv()
+        @pl.loop(0, n_sp - 1)
+        def _(j):
+            slot = nearest(j)
+
+            @pl.when(jnp.logical_not(jnp.logical_and(takes, slot == 0) if relayed else z < 0))
+            def _():
+                merge(slot)
+
     with SC("kv_a"):
         kv_hop(last, 1, False, (CHUNKS - 1,))
         for block in range(1, last):
             kv_hop(block, 1, False)
-        kv_hop(0, 2)
-    top = stat_recv[0, 0:1]
-    for slot in range(1, n_sp):
-        top = jnp.maximum(top, stat_recv[slot, 0:1])
-    weight_sum = jnp.zeros_like(top)
-    weighted = jnp.zeros(run_out.shape[1:], F32)
-    for slot in range(n_sp):
-        share = jnp.exp2((stat_recv[slot, 0:1] - top) * EXP_SCALE) * stat_recv[slot, 1:2]
-        weight_sum = weight_sum + share
-        weighted = weighted + mix_recv[slot].astype(F32) * share
+        kv_hop(0, 2, True, range(lead, CHUNKS))
+        kv_hop(last, 2, True, range(CHUNKS - 1))
     loads[5].wait()
     with SC("rs0"):
-        mixed = scatter_sum(0, head_rows(weighted / weight_sum), out_first)
+        mixed = scatter_sum(0, head_rows(run_out[z] / run_sum[z]), out_first)
     after_first = target_v[...].astype(F32) + normed(mixed, post_first[...])
     stream[...] = after_first
 
@@ -526,8 +623,10 @@
 
     gather_start(1, ffn_input)
     with SC("kv_b"):
-        for block in range(1, n_chip):
+        for block in range(1, last):
             kv_hop(block, 2)
+        kv_hop(0, 3, True, range(lead))
+        kv_hop(last, 2, True, (CHUNKS - 1,))
 
     def halo_rows():
         @pl.when(z > 0)
@@ -559,7 +658,8 @@
         ).astype(BF16)
         loads[8].wait()
     with SC("kv_c"):
-        kv_hop(0, 3)
+        kv_hop(0, 3, True, range(lead, CHUNKS))
+        kv_hop(last, 3, True, range(CHUNKS - 1))
     with SC("rs1"):
         ffn_sum = scatter_sum(1, gated, w_down)
     after_ffn = stream[...] + normed(ffn_sum, ffn_post[...])
@@ -567,8 +667,9 @@
 
     gather_start(2, normed(after_ffn, pre_second[...]))
     with SC("kv_d"):
-        for block in range(1, n_chip):
+        for block in range(1, last):
             kv_hop(block, 3)
+        kv_hop(last, 3, True, (CHUNKS - 1,))
     with SC("ag2_q"):
         loads[9].wait()
         queries = head_columns(gather_times(2, [query_second])[0])
@@ -576,9 +677,6 @@
             q_copy(d, None).wait_send()
         q_slots[z] = queries
 
-    with SC("attn2_own"):
-        absorb(second_rows(z, 0), second_rows(z, 1), q_slots[z], 0, True)
-
     def kv_rest():
         @pl.loop(4, max(n_sp, 4) + 1)
         def _(hop):
@@ -589,15 +687,21 @@
         slot = nearest(j)
         absorb(second_rows(slot, 0), second_rows(slot, 1), q_slots[z], 0, False)
 
-    with SC("attn2_rest"):
+    with SC("attn2"):
         if n_sp > 4:
+            absorb(second_rows(z, 0), second_rows(z, 1), q_slots[z], 0, True)
             kv_rest()
-        times(0, n_sp - 2, absorb_second)
-    with SC("kv_e"):
-        if n_sp <= 4:
-            kv_rest()
-    with SC("attn2_last"):
-        absorb_second(n_sp - 2)
+            times(0, n_sp - 1, absorb_second)
+        else:
+            slots = [z] + [nearest(j) for j in range(n_sp - 1)]
+            scores = dot(second_rows(z, 0), q_slots[z])
+            for index, slot in enumerate(slots):
+                if index == n_sp - 2:
+                    kv_rest()
+                if index < n_sp - 1:
+                    ahead = dot(second_rows(slots[index + 1], 0), q_slots[z])
+                absorb_scores(scores, second_rows(slot, 1), 0, index == 0)
+                scores = ahead
 
     with SC("rs2"):
         loads[10].wait()
@@ -616,10 +720,20 @@
     def drain(d):
         for block in range(n_chip):
             kv_drain(block, d)
-        for copy in mix_copies(sp_at(d), z):
-            copy.wait_send()
+        relay = jnp.logical_and(gives, sp_at(d) == end) if relayed else z < 0
+
+        @pl.when(jnp.logical_not(relay))
+        def _():
+            for copy in mix_copies(sp_at(d), z):
+                copy.wait_send()
 
     times(1, n_sp, drain)
+    if relayed:
+
+        @pl.when(gives)
+        def _():
+            for copy in relay_copies():
+                copy.wait_send()
 
     @pl.when(gives_halo)
     def _():
@@ -694,6 +808,9 @@
         pltpu.VMEM((2, width), BF16),
         dma((2,)),
         pltpu.VMEM((rows, width), F32),
+        pltpu.VMEM((HEAD, columns), BF16),
+        pltpu.VMEM((2, columns), F32),
+        dma((2, 2)),
     ]
 
     def kernel(*refs):

time: 84.1 us -> 81.7 us (0.971)
  Pallas kernels: 83.2 us -> 80.8 us
    pallas_call x1, Pallas kernels: 83.2 us -> 80.8 us  [per_device(): pl.pallas_call(kernel, out_shape=pltpu.VMEM((rows, width), F32), in_specs...]
where the time goes in v3:
time: 81.7 us; the launch traced here: 81.5 us
  Pallas kernels  80.8 us (99%)
    pallas_call x1, Pallas kernels, per_device(): pl.pallas_call(kernel, out_shape=pltpu.VMEM((rows, width), F32), in_specs...  80.8 us

profile of v3, /device:TPU:0, one launch (start us, length us, event | category | flops | bytes accessed | tf_op | source)
XLA Modules:
  0.0 81.5 jit_solution(8501485215934478342)
XLA Ops:
  0.0 80.8 %decoder.1 = f32[32,2048]{1,0:T(8,128)S(1)} custom-call(bf16[32,2048]{1,0:T(8,128)(2,1)} %refs_0_.1, bf16[256,2048]{1,0:T(8,128)(2,1)} %refs_1_.1, f32[1,2048]{1,0:T(1,128)} %bitcast.11, f32[1,2048]{1,0:T(1,128)} %bitcast.12, bf16[2048,512]{1,0:T(8,128)(2,1)} %refs_4_.1, bf16[2048,256]{1,0:T(8,128)(2,1)} %refs_5_.1, bf16[512,2048]{1,0:T(8,128)(2,1)} %refs_6_.1, ...), custom_call_target="tpu_custom_call" | custom-call | tf_op jit(solution)/shard_map/decoder/pallas_call | solution.py:819
  80.8 0.7 copy.22

commit v4 on v3

--- a/solution.py
+++ b/solution.py
@@ -71,7 +71,6 @@
     ffn_post,
     pre_second,
     post_second,
-    vec_sem,
     target_v,
     source_v,
     query_first,
@@ -165,10 +164,11 @@
         (out_second_h, out_second),
     ]
     loads = [
-        pltpu.make_async_copy(a, b, local_sem.at[i]) for i, (a, b) in enumerate(pairs)
+        pltpu.make_async_copy(a, b, local_sem.at[i])
+        for i, (a, b) in enumerate(pairs)
     ]
     vectors = {
-        name: pltpu.make_async_copy(a, b, vec_sem.at[i])
+        name: pltpu.make_async_copy(a, b, local_sem.at[len(pairs) + i])
         for i, (name, a, b) in enumerate([
             ("pre_first", pre_first_h, pre_first),
             ("source_gain", source_gain_h, source_gain),
@@ -206,17 +206,17 @@
     with SC("barrier"):
         pl.semaphore_wait(barrier, n_tp - 1 + n_sp - 1 + jnp.where(gives_halo, n_tp - 1, 0))
 
-    def hidden_copy(phase, piece, slot, device):
+    def hidden_copy(phase, piece, slot, device, index=0):
         return to_tp(
             hidden.at[phase, piece, slot], hidden.at[phase, piece, slot],
-            hidden_send.at[phase], hidden_recv.at[phase, piece, slot], device,
+            hidden_send, hidden_recv.at[phase, piece, index], device,
         )
 
     def gather_start(phase, value):
         for piece in range(PIECES):
             hidden[phase, piece, me] = value[:, piece * span : (piece + 1) * span].astype(BF16)
             for d in range(1, n_chip):
-                hidden_copy(phase, piece, me, tp_at(2 * d)).start()
+                hidden_copy(phase, piece, me, tp_at(2 * d), n_chip - d).start()
             hidden_copy(phase, piece, me, sib).start()
 
     def gather_times(phase, weights, extra=None):
@@ -225,14 +225,13 @@
             if piece < PIECES:
                 for d in range(1, n_chip):
                     slot = tp_at(2 * d)
-                    hidden_copy(phase, piece, slot, sib).wait_recv()
+                    hidden_copy(phase, piece, slot, sib, d).wait_recv()
                     hidden_copy(phase, piece, slot, sib).start()
             if piece == 0:
                 continue
             ready = piece - 1
-            for d in range(n_chip):
-                slot = lax.rem(sib + 2 * d, n_tp)
-                hidden_copy(phase, ready, slot, sib).wait_recv()
+            both = hidden.at[phase, ready, pl.ds(0, n_chip)]
+            pltpu.make_async_copy(both, both, hidden_recv.at[phase, ready, 0]).wait()
             whole = hidden[phase, ready]
             if rows % 16:
                 whole = whole.astype(F32).reshape(block_rows, span).astype(BF16)
@@ -255,14 +254,14 @@
     def pair_copy(phase, piece):
         return to_tp(
             part.at[phase, piece, 1 - core], pair_recv.at[phase, piece],
-            part_send.at[phase, 0], pair_sem.at[phase, piece], sib,
-        )
-
-    def chip_copy(phase, piece, distance, slot):
+            part_send.at[0], pair_sem.at[phase, piece], sib,
+        )
+
+    def chip_copy(phase, piece, distance, slot, index):
         other = lax.rem(chip + distance, n_chip)
         return to_tp(
             pair_sum.at[phase, piece, other], part_recv.at[phase, piece, slot],
-            part_send.at[phase, 1], part_sem.at[phase, piece, slot], 2 * other + core,
+            part_send.at[1], part_sem.at[phase, piece, index], 2 * other + core,
         )
 
     def scatter_sum(phase, left, weight):
@@ -277,13 +276,13 @@
             mine = part[phase, piece, core].astype(F32)
             pair_sum[phase, piece] = (mine + pair_recv[phase, piece].astype(F32)).astype(BF16)
             for d in range(1, n_chip):
-                chip_copy(phase, piece, d, chip).start()
+                chip_copy(phase, piece, d, chip, n_chip - d - 1).start()
         sums = []
         for piece in range(PIECES):
             total = pair_sum[phase, piece, chip].astype(F32)
             for d in range(1, n_chip):
                 slot = lax.rem(chip + d, n_chip)
-                chip_copy(phase, piece, d, slot).wait_recv()
+                chip_copy(phase, piece, d, slot, d - 1).wait_recv()
                 total = total + part_recv[phase, piece, slot].astype(F32)
             sums.append(total)
         return jnp.concatenate(sums, axis=1)
@@ -292,7 +291,7 @@
         for piece in range(PIECES):
             pair_copy(phase, piece).wait_send()
             for d in range(1, n_chip):
-                chip_copy(phase, piece, d, chip).wait_send()
+                chip_copy(phase, piece, d, chip, d - 1).wait_send()
 
     def head_columns(queries):
         blocks = [
@@ -311,17 +310,15 @@
     with SC("norm0"):
         gather_start(0, normed(target_v[...], pre_first[...]))
 
-    def src_copy(slot, c, device, kind):
-        return to_tp(
-            src.at[slot, c], src.at[slot, c], src_send.at[kind], src_recv.at[slot, c], device
-        )
+    def src_copy(slot, c, device, index):
+        return to_tp(src.at[slot, c], src.at[slot, c], src_send, src_recv.at[index, c], device)
 
     loads[1].wait()
     vectors["source_gain"].wait()
     for c in range(CHUNKS):
         src[me, c] = normed(source_v[pl.ds(c * chunk, chunk)], source_gain[...]).astype(BF16)
         for d in range(1, n_chip):
-            src_copy(me, c, tp_at(2 * d), 0).start()
+            src_copy(me, c, tp_at(2 * d), n_chip - d).start()
         src_copy(me, c, sib, 0).start()
 
     def project_pair(block, c, mine, other, layers=(0, 1)):
@@ -361,9 +358,23 @@
         def _(slot):
             absorb(k_first[block], v_first[block], q_slots[slot], slot, fresh)
 
-    def kv_copy(block, slot, c, peer):
+    last = n_chip - 1
+    lead = CHUNKS // 2
+
+    def kv_copy(block, slot, c, peer, receiver):
         held = kv_second.at[slot, block, c]
-        return to_sp(held, held, kv_send, kv_recv.at[slot, block, c], peer)
+        index = slot - jnp.where(slot > receiver, 1, 0)
+        group = int(c >= (lead if block == 0 else CHUNKS - 1))
+        return to_sp(held, held, kv_send, kv_recv.at[index, block, group], peer)
+
+    def kv_wait(block, slot, chunks):
+        edge = lead if block == 0 else CHUNKS - 1
+        index = slot - jnp.where(slot > z, 1, 0)
+        for group in range(2):
+            count = sum(int(c >= edge) == group for c in chunks)
+            if count:
+                held = kv_second.at[slot, block, pl.ds(edge * group, count)]
+                pltpu.make_async_copy(held, held, kv_recv.at[index, block, group]).wait()
 
     def kv_hop(block, hop, arrive=True, chunks=range(CHUNKS)):
         for step in (1, -1):
@@ -373,13 +384,12 @@
             @pl.when(jnp.logical_and(slot >= 0, slot < n_sp))
             def _():
                 if arrive:
-                    for c in chunks:
-                        kv_copy(block, slot, c, sp_at(1)).wait_recv()
+                    kv_wait(block, slot, chunks)
 
                 @pl.when(jnp.logical_and(hop < n_sp, jnp.logical_and(peer >= 0, peer < n_sp)))
                 def _():
                     for c in chunks:
-                        kv_copy(block, slot, c, peer).start()
+                        kv_copy(block, slot, c, peer, peer).start()
 
     def kv_drain(block, hop):
         for step in (1, -1):
@@ -390,7 +400,7 @@
             @pl.when(jnp.logical_and(inside, jnp.logical_and(peer >= 0, peer < n_sp)))
             def _():
                 for c in range(CHUNKS):
-                    kv_copy(block, slot, c, peer).wait_send()
+                    kv_copy(block, slot, c, peer, peer).wait_send()
 
     def nearest(j):
         up = j + jnp.where(j >= z, 1, 0)
@@ -415,23 +425,21 @@
     def q_copy(distance, slot):
         return to_sp(
             q_slots.at[z], q_slots.at[z] if slot is None else q_slots.at[slot],
-            q_sem.at[0, 0], q_sem.at[1, z if slot is None else slot], sp_at(distance),
+            q_sem.at[0], q_sem.at[1], sp_at(distance),
         )
 
     for d in range(1, n_sp):
         q_copy(d, None).start()
 
-    last = n_chip - 1
-    lead = CHUNKS // 2
 
     def near_chunk(d, c):
         near = tp_at(2 * d)
-        src_copy(near, c, sib, 1).wait_recv()
-        src_copy(near, c, sib, 1).start()
+        src_copy(near, c, sib, d).wait_recv()
+        src_copy(near, c, sib, n_chip - 1 + d).start()
 
     def far_chunk(d, c, layers=(0, 1)):
         far = lax.rem(sib + 2 * d, n_tp)
-        src_copy(far, c, sib, 1).wait_recv()
+        src_copy(far, c, sib, n_chip - 1 + d).wait_recv()
         project_pair(d, c, tp_at(2 * d), far, layers)
 
     def absorb_chunks(low, high):
@@ -450,8 +458,8 @@
         with SC("lead"):
             lead_chunks()
     with SC("qwait"):
-        for d in range(1, n_sp):
-            q_copy(d, sp_at(d)).wait_recv()
+        others = q_slots.at[pl.ds(0, n_sp - 1)]
+        pltpu.make_async_copy(others, others, q_sem.at[1]).wait()
     kv_hop(0, 1, False, range(lead, CHUNKS))
     kv_hop(0, 2, True, range(lead))
     with SC("abs_own"):
@@ -485,7 +493,7 @@
 
     def mix_copies(peer, slot):
         return [
-            to_sp(sent.at[peer], got.at[slot], mix_sem.at[index, 0, 0], mix_sem.at[index, 1, slot], peer)
+            to_sp(sent.at[peer], got.at[slot], mix_sem.at[index, n_sp], mix_sem.at[index, slot], peer)
             for index, (sent, got) in enumerate(((mix_send, mix_recv), (stat_send, stat_recv)))
         ]
 
@@ -549,8 +557,8 @@
         finish_slot(z)
         project_pair(last, CHUNKS - 1, tp_at(2 * last), lax.rem(sib + 2 * last, n_tp), (1,))
     with SC("transpose"):
-        loads[6].wait()
-        loads[7].wait()
+        for load in loads[5:]:
+            load.wait()
         for name in list(vectors)[2:]:
             vectors[name].wait()
         stripe = 2 * HEAD
@@ -601,7 +609,6 @@
             kv_hop(block, 1, False)
         kv_hop(0, 2, True, range(lead, CHUNKS))
         kv_hop(last, 2, True, range(CHUNKS - 1))
-    loads[5].wait()
     with SC("rs0"):
         mixed = scatter_sum(0, head_rows(run_out[z] / run_sum[z]), out_first)
     after_first = target_v[...].astype(F32) + normed(mixed, post_first[...])
@@ -656,7 +663,6 @@
             jax.nn.gelu(causal_mix(up_gate, conv_gate[...]), approximate=True)
             * causal_mix(up_value, conv_value[...])
         ).astype(BF16)
-        loads[8].wait()
     with SC("kv_c"):
         kv_hop(0, 3, True, range(lead, CHUNKS))
         kv_hop(last, 3, True, range(CHUNKS - 1))
@@ -671,7 +677,6 @@
             kv_hop(block, 3)
         kv_hop(last, 3, True, (CHUNKS - 1,))
     with SC("ag2_q"):
-        loads[9].wait()
         queries = head_columns(gather_times(2, [query_second])[0])
         for d in range(1, n_sp):
             q_copy(d, None).wait_send()
@@ -704,7 +709,6 @@
                 scores = ahead
 
     with SC("rs2"):
-        loads[10].wait()
         mixed = scatter_sum(2, head_rows(run_out[0] / run_sum[0]), out_second)
     decoded[...] = stream[...] + normed(mixed, post_second[...])
 
@@ -769,26 +773,26 @@
     line = pltpu.VMEM((1, width), F32)
     scratch = [
         *([line] * 4), pltpu.VMEM(conv_gate.shape, F32), pltpu.VMEM(conv_value.shape, F32),
-        *([line] * 3), dma((9,)),
+        *([line] * 3),
         pltpu.VMEM(target.shape, BF16),
         pltpu.VMEM(source.shape, BF16),
         *(pltpu.VMEM(w.shape, BF16) for w in (
             query_first, keyval_first, out_first, w_gate.T, w_value.T, w_gate, w_value, w_down,
             query_second, keyval_second, out_second)),
-        dma((11,)),
+        dma((20,)),
         pltpu.VMEM((3, PIECES, n_tp, rows, span), BF16),
-        dma((3,)),
-        dma((3, PIECES, n_tp)),
+        dma,
+        dma((3, PIECES, n_chip)),
         pltpu.VMEM((n_tp, CHUNKS, lines // CHUNKS, width), BF16),
+        dma,
+        dma((2 * n_chip - 1, CHUNKS)),
+        pltpu.VMEM((n_sp, HEAD, columns), BF16),
         dma((2,)),
-        dma((n_tp, CHUNKS)),
-        pltpu.VMEM((n_sp, HEAD, columns), BF16),
-        dma((2, n_sp)),
         pltpu.VMEM((n_chip, 2 * lines, HEAD), BF16),
         pltpu.VMEM((n_chip, 2 * lines, HEAD), BF16),
         pltpu.VMEM((n_sp, n_chip, CHUNKS, 2, 2 * lines // CHUNKS, HEAD), BF16),
         dma,
-        dma((n_sp, n_chip, CHUNKS)),
+        dma((n_sp - 1, n_chip, 2)),
         pltpu.VMEM((n_sp, 1, columns), F32),
         pltpu.VMEM((n_sp, 1, columns), F32),
         pltpu.VMEM((n_sp, HEAD, columns), F32),
@@ -796,14 +800,14 @@
         pltpu.VMEM((n_sp, HEAD, columns), BF16),
         pltpu.VMEM((n_sp, 2, columns), F32),
         pltpu.VMEM((n_sp, 2, columns), F32),
-        dma((2, 2, n_sp)),
+        dma((2, n_sp + 1)),
         pltpu.VMEM((3, PIECES, 2, n_chip, rows, span), BF16),
         pltpu.VMEM((3, PIECES, n_chip, rows, span), BF16),
         pltpu.VMEM((3, PIECES, n_chip, rows, span), BF16),
         pltpu.VMEM((3, PIECES, n_chip, rows, span), BF16),
-        dma((3, 2)),
+        dma((2,)),
         dma((3, PIECES)),
-        dma((3, PIECES, n_chip)),
+        dma((3, PIECES, n_chip - 1)),
         pltpu.VMEM((2, width), BF16),
         pltpu.VMEM((2, width), BF16),
         dma((2,)),

time: 81.7 us -> 81.1 us (level)
  no operation moved by 1% of the time
where the time goes in v4:
time: 81.1 us; the launch traced here: 80.9 us
  Pallas kernels  80.2 us (99%)
    pallas_call x1, Pallas kernels, per_device(): pl.pallas_call(kernel, out_shape=pltpu.VMEM((rows, width), F32), in_specs...  80.2 us

profile of v4, /device:TPU:0, one launch (start us, length us, event | category | flops | bytes accessed | tf_op | source)
XLA Modules:
  0.0 80.9 jit_solution(8572999123960760629)
XLA Ops:
  0.0 80.2 %decoder.1 = f32[32,2048]{1,0:T(8,128)S(1)} custom-call(bf16[32,2048]{1,0:T(8,128)(2,1)} %refs_0_.1, bf16[256,2048]{1,0:T(8,128)(2,1)} %refs_1_.1, f32[1,2048]{1,0:T(1,128)} %bitcast.11, f32[1,2048]{1,0:T(1,128)} %bitcast.12, bf16[2048,512]{1,0:T(8,128)(2,1)} %refs_4_.1, bf16[2048,256]{1,0:T(8,128)(2,1)} %refs_5_.1, bf16[512,2048]{1,0:T(8,128)(2,1)} %refs_6_.1, ...), custom_call_target="tpu_custom_call" | custom-call | tf_op jit(solution)/shard_map/decoder/pallas_call | solution.py:823
  80.2 0.7 copy.22
